TPU v7x, 512 devices: a 8x2x16 block of a 8x8x16 slice. The times are simulated.
512 devices in a mesh: grp: 2 (over y), sp: 16 (over z), tp: 16 (over x, core).
Axes of the slice: x: 8, y: 2, z: 16, core: 2. Of those that a mesh axis runs over, the one named last changes fastest.
The devices are a block of a 8x8x16 slice.
Arguments:
- latent: bfloat16 [16384, 4096], P(('grp', 'sp'), 'tp'), parts along dimension 0, may hold values from -42 to 42
- context: bfloat16 [2048, 4096], P(('grp', 'sp'), 'tp'), parts along dimension 0, may hold values from -42 to 42
- conditions: float32 [4, 4096], P('grp', 'sp'), parts along dimension 0, may hold values from -6 to 6
- mod_weight: bfloat16 [4096, 3, 4096], P('sp', None, 'tp'), may hold values from -0.09375 to 0.09375
- norm_gain: float32 [4096], P('tp'), may hold values from 0.1 to 1.9
- w_query: bfloat16 [4096, 2048], P(None, 'tp'), may hold values from -0.09375 to 0.09375
- w_key: bfloat16 [4096, 2048], P(None, 'tp'), may hold values from -0.09375 to 0.09375
- w_value: bfloat16 [4096, 2048], P(None, 'tp'), may hold values from -0.09375 to 0.09375
- query_gain: float32 [64], replicated, may hold values from 1 to 14
- key_gain: float32 [64], replicated, may hold values from 1 to 14
- lambdas: float32 [16], P('tp'), may hold values from 0.3 to 0.8
- out_gain: float32 [128], replicated, may hold values from 0.1 to 1.9
- w_out: bfloat16 [2048, 4096], P(None, 'tp'), may hold values from -0.125 to 0.125
Outputs:
- updated: bfloat16 [16384, 4096], P(('grp', 'sp'), 'tp'), parts along dimension 0
There are 2 independent parts, one for each index of `grp`. A program takes and returns all parts, laid end to end along the dimension named above; an argument that names none is the same for every part. Nothing has to cross between parts.
All inputs are finite; a program needn't handle non-finite values.
Results may differ from a plain program's by a relative error of at most 0.0076.
Values may be sent and summed in bfloat16 or wider, within the bound.
A program may use at most 64 MiB of HBM per device.

v0:
```python
import math
import jax
import jax.numpy as jnp
from jax import lax
from jax.sharding import PartitionSpec as P

DK = 64
DV = 128
GRID_W = 64
epsilon = 1e-06


def sent_to_all(value, axis):
    size = lax.axis_size(axis)
    return lax.all_to_all(
        jnp.broadcast_to(value[None], (size, *value.shape)), axis, 0, 0, tiled=True
    )


def of_everyone(value, axis):
    everything = sent_to_all(value, axis)
    return jnp.sum(everything, axis=0)


def in_one_piece(arrays, axis, dim, along):
    both = jnp.concatenate(arrays, axis=along)
    whole, at, gathered = (lax.all_gather(both, axis, axis=dim, tiled=True), 0, [])
    for a in arrays:
        gathered.append(lax.slice_in_dim(whole, at, at + a.shape[along], axis=along))
        at += a.shape[along]
    return tuple(gathered)


def turn_half(halves, angles):
    quarter = halves.shape[-1] // 2
    cosine = jnp.cos(angles)[:, None, None, :]
    sine_part = jnp.sin(angles)[:, None, None, :]
    first_part = halves[..., :quarter]
    second = halves[..., quarter:]
    return jnp.concatenate(
        [first_part * cosine - second * sine_part, first_part * sine_part + second * cosine],
        axis=-1,
    )


def rotate(features, positions):
    half_width = features.shape[-1] // 2
    quarter = half_width // 2
    inverse = 10000.0 ** (-2.0 * jnp.arange(quarter, dtype=jnp.float32) / half_width)
    grid_row = (positions // GRID_W).astype(jnp.float32)
    grid_column = (positions % GRID_W).astype(jnp.float32)
    return jnp.concatenate(
        [
            turn_half(features[..., :half_width], grid_row[:, None] * inverse),
            turn_half(features[..., half_width:], grid_column[:, None] * inverse),
        ],
        axis=-1,
    )


def head_norm(features, gain_row):
    return (
        features
        * lax.rsqrt(jnp.mean(features * features, axis=-1, keepdims=True) + epsilon)
        * gain_row
    )


def modulate(rows_in, gain_row, shift_row, scale_row):
    floats = rows_in.astype(jnp.float32)
    factor = lax.rsqrt(jnp.mean(floats * floats, axis=1, keepdims=True) + epsilon)
    return (floats * factor * gain_row * (1.0 + scale_row) + shift_row).astype(jnp.bfloat16)


def local(
    latent,
    context,
    conditions,
    mod_weight,
    norm_gain,
    w_query,
    w_key,
    w_value,
    query_gain,
    key_gain,
    lambdas,
    out_gain,
    w_out,
):
    tok_rows = latent.shape[0]
    ctx_rows = context.shape[0]
    columns = latent.shape[1]
    heads_here = lambdas.shape[0]
    in_rows = mod_weight.shape[0]
    activated = jax.nn.silu(conditions).astype(jnp.bfloat16)
    partial_mod = jnp.dot(
        activated, mod_weight.reshape(in_rows, 3 * columns), preferred_element_type=jnp.float32
    ).reshape(2, 3, columns)
    modulation = of_everyone(partial_mod, "sp")
    lat_floats = latent.astype(jnp.float32)
    full_gain, full_pairs = (
        lax.all_gather(norm_gain, "tp", axis=0, tiled=True),
        lax.all_gather(modulation[:, :2], "tp", axis=2, tiled=True),
    )
    whole_lat, whole_ctx = in_one_piece((latent, context), "tp", 1, 0)
    hidden = modulate(whole_lat, full_gain, full_pairs[0, 0], full_pairs[0, 1])
    hidden_ctx = modulate(whole_ctx, full_gain, full_pairs[1, 0], full_pairs[1, 1])
    query_raw = jnp.dot(hidden, w_query, preferred_element_type=jnp.float32)
    key_raw = jnp.dot(hidden, w_key, preferred_element_type=jnp.float32)
    value_raw = jnp.dot(hidden, w_value, preferred_element_type=jnp.float32)
    ctx_key_raw = jnp.dot(hidden_ctx, w_key, preferred_element_type=jnp.float32)
    ctx_value_raw = jnp.dot(hidden_ctx, w_value, preferred_element_type=jnp.float32)
    positions = lax.axis_index("sp") * tok_rows + jnp.arange(tok_rows, dtype=jnp.int32)
    queries = rotate(
        head_norm(query_raw.reshape(tok_rows, heads_here, 2, DK), query_gain), positions
    ).astype(jnp.bfloat16)
    lat_keys = (
        rotate(head_norm(key_raw.reshape(tok_rows, heads_here, 2, DK), key_gain), positions)
        .astype(jnp.bfloat16)
        .reshape(tok_rows, heads_here * 2 * DK)
    )
    lat_values = value_raw.astype(jnp.bfloat16)
    ctx_keys = (
        head_norm(ctx_key_raw.reshape(ctx_rows, heads_here, 2, DK), key_gain)
        .astype(jnp.bfloat16)
        .reshape(ctx_rows, heads_here * 2 * DK)
    )
    ctx_values = ctx_value_raw.astype(jnp.bfloat16)
    scaling = DK ** (-0.5)

    def absorb(carried, key_rows, value_rows):
        key_count = key_rows.shape[0]
        key_block = key_rows.reshape(key_count, heads_here, 2, DK)
        value_block = value_rows.reshape(key_count, heads_here, DV)
        running_max, totals, weighted = carried
        scores = (
            jnp.einsum("qhmd,khmd->qhmk", queries, key_block, preferred_element_type=jnp.float32)
            * scaling
        )
        new_max = jnp.maximum(running_max, jnp.max(scores, axis=-1))
        rescale = jnp.exp(running_max - new_max)
        exponent = jnp.exp(scores - new_max[..., None])
        totals = totals * rescale + jnp.sum(exponent, axis=-1)
        weighted = weighted * rescale[..., None] + jnp.einsum(
            "qhmk,khv->qhmv",
            exponent.astype(jnp.bfloat16),
            value_block,
            preferred_element_type=jnp.float32,
        )
        return (new_max, totals, weighted)

    def absorb_rows(carried, key_rows, value_rows):
        key_count = key_rows.shape[0]
        block_rows = math.gcd(key_count, 512)

        def visit_block(block_index, partial_value):
            first_row = block_index * block_rows
            return absorb(
                partial_value,
                lax.dynamic_slice_in_dim(key_rows, first_row, block_rows, 0),
                lax.dynamic_slice_in_dim(value_rows, first_row, block_rows, 0),
            )

        return lax.fori_loop(0, key_count // block_rows, visit_block, carried)

    initial_state = (
        jnp.full((tok_rows, heads_here, 2), -1e30, jnp.float32),
        jnp.zeros((tok_rows, heads_here, 2), jnp.float32),
        jnp.zeros((tok_rows, heads_here, 2, DV), jnp.float32),
    )
    every_ctx_keys, every_ctx_values = in_one_piece((ctx_keys, ctx_values), "sp", 0, 1)
    carried = absorb_rows(initial_state, every_ctx_keys, every_ctx_values)
    pieces = in_one_piece((lat_keys, lat_values), "sp", 0, 1)
    carried = absorb_rows(carried, pieces[0], pieces[1])
    running_max, totals, weighted = carried
    attended = (
        weighted[:, :, 0] / totals[:, :, 0, None]
        - lambdas[None, :, None] * weighted[:, :, 1] / totals[:, :, 1, None]
    )
    head_out = head_norm(attended, out_gain).astype(jnp.bfloat16).reshape(tok_rows, heads_here * DV)
    mixed_rows = jnp.dot(
        lax.all_gather(head_out, "tp", axis=1, tiled=True),
        w_out,
        preferred_element_type=jnp.float32,
    )
    return (lat_floats + modulation[0, 2] * mixed_rows).astype(jnp.bfloat16)


def solution(mesh):
    in_specs = (
        P(("grp", "sp"), "tp"),
        P(("grp", "sp"), "tp"),
        P("grp", "sp"),
        P("sp", None, "tp"),
        P("tp"),
        P(None, "tp"),
        P(None, "tp"),
        P(None, "tp"),
        P(),
        P(),
        P("tp"),
        P(),
        P(None, "tp"),
    )
    out_specs = P(("grp", "sp"), "tp")
    return jax.shard_map(local, mesh=mesh, in_specs=in_specs, out_specs=out_specs, check_vma=False)
```

profile of v0, /device:TPU:65, one launch (start us, length us, event | category | flops | bytes accessed | tf_op | source)
XLA Modules:
  0.0 304.0 jit_solution(5467779890000573192)
XLA Ops:
  6.6 1.8 pad_maximum_fusion
  11.2 44.2 %all-to-all-start = ((f32[16,2,3,256]{3,1,2,0:T(2,128)}), f32[16,2,3,256]{3,1,2,0:T(2,128)S(1)}, u32[]{:S(2)}, u32[]{:S(2)}) async-start(f32[16,2,3,256]{3,1,2,0:T(2,128)} %broadcast_in_dim.16), calls=%async_computation | async-start | bytes 196608 | tf_op jit(solution)/shard_map/all_to_all | solution.py:15
  55.5 18.9 %all-gather = f32[16,1,256]{2,1,0:T(1,128)S(1)} all-gather(f32[1,1,256]{2,1,0:T(1,128)S(1)} %bitcast.220), channel_id=1, replica_groups=mesh['grp'=2,'sp'=16,'tp'=16] {'tp'}, dimensions={0}, use_global_device_ids=true | all-gather | bytes 17408 | tf_op jit(solution)/shard_map/all_gather | solution.py:102
  74.8 15.3 %all_gather.20 = f32[2,2,4096]{2,0,1:T(2,128)S(1)} all-gather(f32[2,2,256]{2,0,1:T(2,128)S(1)} %slice.110), channel_id=1, replica_groups=mesh['grp'=2,'sp'=16,'tp'=16] {'tp'}, dimensions={2}, use_global_device_ids=true | all-gather | bytes 69632 | tf_op jit(solution)/shard_map/all_gather | solution.py:103
  90.2 13.1 %all-gather.5.cloned.1.call-done = bf16[576,4096]{1,0:T(8,128)(2,1)} async-done(((bf16[576,256]{1,0:T(8,128)(2,1)}), bf16[576,4096]{1,0:T(8,128)(2,1)}) %all-gather.5.cloned.1.call-update) | async-done | bytes 4718608 | tf_op jit(solution)/shard_map/all_gather | solution.py:27
  103.3 3.1 %fusion.30 = f32[512]{0:T(512)S(1)} fusion(bf16[576,4096]{1,0:T(8,128)(2,1)} %all-gather.5.cloned.1.call-done), kind=kLoop, calls=%fused_computation.47 | loop fusion | flops 6290944 | bytes 4196352 | tf_op jit(solution)/shard_map/reduce_sum | solution.py:71
  106.4 3.4 %fusion.34 = bf16[512,4096]{1,0:T(8,128)(2,1)S(1)} fusion(f32[4096]{0:T(1024)S(1)} %bitcast.211, f32[4096]{0:T(1024)S(1)} %bitcast.210, f32[4096]{0:T(1024)S(1)} %bitcast.207, f32[512]{0:T(512)S(1)} %add_rsqrt_fusion.4, bf16[576,4096]{1,0:T(8,128)(2,1)} %all-gather.5.cloned.1.call-done), kind=kLoop, calls=%fused_computation.51 | loop fusion | flops 12582912 | bytes 8439808 | tf_op jit(solution)/shard_map/convert_element_type | solution.py:72
  109.8 1.5 convolution_convert_fusion
  116.5 1.8 fusion.66
  118.8 1.5 convolution_convert_fusion.1
  120.4 3.7 %fusion.67 = f32[512,128]{0,1:T(8,128)S(1)} fusion(bf16[512,4096]{1,0:T(8,128)(2,1)} %copy-done.1, bf16[4096,128]{1,0:T(8,128)(2,1)S(1)} %copy-done.4), kind=kOutput, calls=%fused_computation.130 | convolution fusion | flops 536870912 | bytes 5505024 | tf_op jit(solution)/shard_map/dot_general | solution.py:108
  124.3 29.9 %all_gather.21 = bf16[1024,256]{1,0:T(8,128)(2,1)S(1)} all-gather(bf16[64,256]{1,0:T(8,128)(2,1)S(1)} %pad_maximum_fusion.4), channel_id=1, replica_groups=mesh['grp'=2,'sp'=16,'tp'=16] {'sp'}, dimensions={0}, use_global_device_ids=true | all-gather | bytes 557056 | tf_op jit(solution)/shard_map/all_gather | solution.py:27
  154.2 3.5 %while.36 = (s32[]{:T(128)}, f32[512,1,2]{0,2,1:T(2,128)S(1)}, f32[512,1,2]{0,2,1:T(2,128)S(1)}, f32[512,1,2,128]{0,3,2,1:T(8,128)S(1)}, bf16[1024,128]{1,0:T(8,...) while((s32[]{:T(128)}, f32[512,1,2]{0,2,1:T(2,128)S(1)}, ...), condition=%wide.region_8.9_spmd.clone, body=%wide.region_5.8_spmd.clone.sunk | while | flops 205920256 | bytes 8323255 | solution.py:164
  157.7 28.5 %all-gather.7.cloned.1.call-done = bf16[8192,256]{0,1:T(8,128)(2,1)} async-done(((bf16[512,256]{0,1:T(8,128)(2,1)}), bf16[8192,256]{0,1:T(8,128)(2,1)}) %all-gather.7.cloned.1.call-update) | async-done | bytes 4194320 | tf_op jit(solution)/shard_map/all_gather | solution.py:27
  186.2 4.6 %fusion.63 = (bf16[8192,128]{0,1:T(8,128)(2,1)}, bf16[8192,128]{0,1:T(8,128)(2,1)}) fusion(bf16[8192,256]{0,1:T(8,128)(2,1)} %all-gather.7.cloned.1.call-done), kind=kLoop, calls=%fused_computation.126 | loop fusion | bytes 8388608 | tf_op jit(solution)/shard_map/slice | solution.py:29
  190.8 54.4 %while.35 = (s32[]{:T(128)}, f32[512,1,2]{0,2,1:T(2,128)S(1)}, f32[512,1,2]{0,2,1:T(2,128)S(1)}, f32[512,1,2,128]{0,3,2,1:T(8,128)S(1)}, bf16[8192,128]{0,1:T(8,...) while((s32[]{:T(128)}, f32[512,1,2]{0,2,1:T(2,128)S(1)}, ...), condition=%wide.region_13.14_spmd, body=%wide.region_10.13_spmd.sunk | while | flops 205786112 | bytes 8061091 | solution.py:164
  192.7 1.5 fusion.98
  196.1 1.5 fusion.98
  199.5 1.5 fusion.98
  202.9 1.5 fusion.98
  206.3 1.5 fusion.98
  209.7 1.5 fusion.98
  213.1 1.5 fusion.98
  216.5 1.5 fusion.98
  219.9 1.5 fusion.98
  223.2 1.5 fusion.98
  230.0 1.5 fusion.98
  233.4 1.5 fusion.98
  236.8 1.5 fusion.98
  243.6 1.5 fusion.98
  246.1 48.3 %all-gather.9.cloned.1.call-done = bf16[512,2048]{0,1:T(8,128)(2,1)} async-done(((bf16[512,128]{0,1:T(8,128)(2,1)}), bf16[512,2048]{0,1:T(8,128)(2,1)}) %all-gather.9.cloned.1.call-update) | async-done | bytes 2097168 | tf_op jit(solution)/shard_map/all_gather | solution.py:182
  294.4 3.1 %fusion.36 = bf16[512,256]{1,0:T(8,128)(2,1)} fusion(bf16[512,2048]{0,1:T(8,128)(2,1)} %all-gather.9.cloned.1.call-done, bf16[2048,256]{1,0:T(8,128)(2,1)S(1)} %copy-done, bf16[512,256]{1,0:T(8,128)(2,1)S(1)} %copy-done.5, f32[256]{0:T(256)S(1)} %bitcast.221), kind=kOutput, calls=%fused_computation.56 | convolution fusion | flops 537395200 | bytes 3671040 | tf_op jit(solution)/shard_map/dot_general | solution.py:181
  (183 shorter events, 44.8 us)
Async XLA Ops:
  6.5 287.9 %copy-start = (bf16[2048,256]{1,0:T(8,128)(2,1)S(1)}, bf16[2048,256]{1,0:T(8,128)(2,1)}, u32[]{:S(2)}) copy-start(bf16[2048,256]{1,0:T(8,128)(2,1)} %param.29) | copy-start | bytes 3145732
  6.6 49.0 %copy-start.6 = (f32[256]{0:T(256)S(1)}, f32[256]{0:T(256)}, u32[]{:S(2)}) copy-start(f32[256]{0:T(256)} %param.21) | copy-start | bytes 3076
  6.6 96.7 %all-gather.5.cloned.1.call-start = ((), (), s32[]{:S(2)}) async-start(), calls=%async_computation.1 | async-start | bytes 5013504 | tf_op jit(solution)/shard_map/all_gather | solution.py:27
  11.2 63.6 %all-to-all-start = ((f32[16,2,3,256]{3,1,2,0:T(2,128)}), f32[16,2,3,256]{3,1,2,0:T(2,128)S(1)}, u32[]{:S(2)}, u32[]{:S(2)}) async-start(f32[16,2,3,256]{3,1,2,0:T(2,128)} %broadcast_in_dim.16), calls=%async_computation | async-start | bytes 196608 | tf_op jit(solution)/shard_map/all_to_all | solution.py:15
  55.4 130.8 %all-gather.7.cloned.1.call-start = ((), (), s32[]{:S(2)}) async-start(), calls=%async_computation.2 | async-start | bytes 4456448 | tf_op jit(solution)/shard_map/all_gather | solution.py:27
  106.4 3.4 %copy-start.2 = (bf16[4096,128]{1,0:T(8,128)(2,1)S(1)}, bf16[4096,128]{1,0:T(8,128)(2,1)}, u32[]{:S(2)}) copy-start(bf16[4096,128]{1,0:T(8,128)(2,1)} %param.24) | copy-start | bytes 3145732
  109.8 2.0 copy-start.1
  109.8 2.0 copy-start.3
  111.8 1.6 copy-start.7
  114.4 180.1 %all-gather.9.cloned.1.call-start = ((), (), s32[]{:S(2)}) async-start(), calls=%async_computation.3 | async-start | bytes 2228224 | tf_op jit(solution)/shard_map/all_gather | solution.py:182
  118.8 1.6 copy-start.4
  120.4 3.8 %copy-start.8 = (f32[64]{0:T(128)S(1)}, f32[64]{0:T(128)}, u32[]{:S(2)}) copy-start(f32[64]{0:T(128)} %param.25) | copy-start | bytes 772
  190.8 54.5 %copy-start.9 = (f32[128]{0:T(128)S(1)}, f32[128]{0:T(128)}, u32[]{:S(2)}) copy-start(f32[128]{0:T(128)} %param.28) | copy-start | bytes 1540
  190.8 103.6 %copy-start.5 = (bf16[512,256]{1,0:T(8,128)(2,1)S(1)}, bf16[512,256]{1,0:T(8,128)(2,1)}, u32[]{:S(2)}) copy-start(bf16[512,256]{1,0:T(8,128)(2,1)} %param.17) | copy-start | bytes 786436
Sparse Core Ops, SparseCore 0:
  9.4 93.8 all-gather.4
  114.5 71.6 all-gather.6
  246.3 48.1 all-gather.8
where the time goes:
time: 305 us; the launch traced here: 304 us
  waiting for transfers between devices  90.1 us (30%)
  blocking collectives  64.1 us (21%)
  matrix products  48.7 us (16%)
  starting transfers between devices  44.4 us (15%)
  local copies, waits for them, and re-layouts  22.5 us (7%)
  other arithmetic  19.2 us (6%)
  between operations  14.1 us (5%)
    all_gather x1, waiting for transfers between devices, local(): lax.all_gather(head_out, 'tp', axis=1, tiled=True)  48.3 us
    all_to_all x1, starting transfers between devices, sent_to_all(): lax.all_to_all(jnp.broadcast_to(value[None], (size, *value.shape)), axis,...  44.2 us
    all_gather x2, waiting for transfers between devices, in_one_piece(): lax.all_gather(both, axis, axis=dim, tiled=True)  41.6 us
    all_gather x1, blocking collectives, in_one_piece(): lax.all_gather(both, axis, axis=dim, tiled=True)  29.9 us
    dot_general x18, matrix products, absorb(): jnp.einsum('qhmk,khv->qhmv', exponent.astype(jnp.bfloat16), value_block,...  25.7 us
    all_gather x1, blocking collectives, local(): lax.all_gather(norm_gain, 'tp', axis=0, tiled=True)  18.9 us
    all_gather x1, blocking collectives, local(): lax.all_gather(modulation[:, :2], 'tp', axis=2, tiled=True)  15.3 us
    dynamic_slice x20, local copies, waits for them, and re-layouts, visit_block(): lax.dynamic_slice_in_dim(key_rows, first_row, block_rows, 0)  15 us
  transfers between devices with their start and end apart: 4, of which 3 were waited for; matrix products, arithmetic and copies ran while one was open for 5% of the time, Pallas kernels for 0%

commit v1 on v0

--- a/solution.py
+++ b/solution.py
@@ -1,3 +1,4 @@
+import functools
 import math
 import jax
 import jax.numpy as jnp
@@ -8,6 +9,21 @@
 DV = 128
 GRID_W = 64
 epsilon = 1e-06
+
+
+def name_positions(local_x, net_axis):
+    return jnp.concatenate(
+        lax.all_to_all(
+            jnp.stack([local_x for _ in range(lax.psum(1, axis_name=net_axis))]),
+            axis_name=net_axis,
+            split_axis=0,
+            concat_axis=0,
+        ),
+        axis=2,
+    )
+
+
+get_case_up = functools.partial(name_positions, net_axis="tp")
 
 
 def sent_to_all(value, axis):
@@ -100,7 +116,7 @@
     lat_floats = latent.astype(jnp.float32)
     full_gain, full_pairs = (
         lax.all_gather(norm_gain, "tp", axis=0, tiled=True),
-        lax.all_gather(modulation[:, :2], "tp", axis=2, tiled=True),
+        get_case_up(modulation[:, :2]),
     )
     whole_lat, whole_ctx = in_one_piece((latent, context), "tp", 1, 0)
     hidden = modulate(whole_lat, full_gain, full_pairs[0, 0], full_pairs[0, 1])

time: 305 us -> 307 us (level)
  blocking collectives: 64.1 us -> 49.9 us
  waiting for transfers between devices: 90.1 us -> 101 us
  starting transfers between devices: 44.4 us -> 48.7 us
    all_gather x1 -> x0, blocking collectives: 15.3 us -> none  [local(): lax.all_gather(modulation[:, :2], 'tp', axis=2, tiled=True)]
    all_to_all x0 -> x1, waiting for transfers between devices: none -> 8.16 us  [name_positions(): lax.all_to_all(jnp.stack([local_x for _ in range(lax.psum(1, axis_name=ne...]
    all_to_all x0 -> x1, starting transfers between devices: none -> 4.36 us  [name_positions(): lax.all_to_all(jnp.stack([local_x for _ in range(lax.psum(1, axis_name=ne...]
  transfers between devices with their start and end apart: 4 -> 5, of which waited for: 3 -> 4; matrix products, arithmetic and copies ran while one was open for 5% -> 5% of each run, Pallas kernels for 0% -> 0%
where the time goes in v1:
time: 307 us; the launch traced here: 306 us
  waiting for transfers between devices  101 us (33%)
  blocking collectives  49.9 us (16%)
  starting transfers between devices  48.7 us (16%)
  matrix products  48.7 us (16%)
  local copies, waits for them, and re-layouts  23.1 us (8%)
  other arithmetic  19.2 us (6%)
  between operations  14.2 us (5%)
    all_gather x1, waiting for transfers between devices, local(): lax.all_gather(head_out, 'tp', axis=1, tiled=True)  48.9 us
    all_to_all x1, starting transfers between devices, sent_to_all(): lax.all_to_all(jnp.broadcast_to(value[None], (size, *value.shape)), axis,...  44.2 us
    all_gather x2, waiting for transfers between devices, in_one_piece(): lax.all_gather(both, axis, axis=dim, tiled=True)  44 us
    all_gather x1, blocking collectives, in_one_piece(): lax.all_gather(both, axis, axis=dim, tiled=True)  31 us
    dot_general x18, matrix products, absorb(): jnp.einsum('qhmk,khv->qhmv', exponent.astype(jnp.bfloat16), value_block,...  25.7 us
    all_gather x1, blocking collectives, local(): lax.all_gather(norm_gain, 'tp', axis=0, tiled=True)  18.9 us
    dynamic_slice x20, local copies, waits for them, and re-layouts, visit_block(): lax.dynamic_slice_in_dim(key_rows, first_row, block_rows, 0)  15 us
    dot_general x18, matrix products, absorb(): jnp.einsum('qhmd,khmd->qhmk', queries, key_block, preferred_element_type=...  9.01 us
  transfers between devices with their start and end apart: 5, of which 4 were waited for; matrix products, arithmetic and copies ran while one was open for 5% of the time, Pallas kernels for 0%

profile of v1, /device:TPU:65, one launch (start us, length us, event | category | flops | bytes accessed | tf_op | source)
XLA Modules:
  0.0 306.1 jit_solution(9176195008581425117)
XLA Ops:
  6.6 1.8 pad_maximum_fusion
  11.2 44.2 %all-to-all-start = ((f32[16,2,3,256]{3,1,2,0:T(2,128)}), f32[16,2,3,256]{3,1,2,0:T(2,128)S(1)}, u32[]{:S(2)}, u32[]{:S(2)}) async-start(f32[16,2,3,256]{3,1,2,0:T(2,128)} %broadcast_in_dim.16), calls=%async_computation | async-start | bytes 196608 | tf_op jit(solution)/shard_map/all_to_all | solution.py:31
  55.5 18.9 %all-gather = f32[16,1,256]{2,1,0:T(1,128)S(1)} all-gather(f32[1,1,256]{2,1,0:T(1,128)S(1)} %bitcast.225), channel_id=1, replica_groups=mesh['grp'=2,'sp'=16,'tp'=16] {'tp'}, dimensions={0}, use_global_device_ids=true | all-gather | bytes 17408 | tf_op jit(solution)/shard_map/all_gather | solution.py:118
  75.1 4.4 %all-to-all-start.1 = ((f32[16,2,2,256]{3,2,1,0:T(2,128)}), f32[16,2,2,256]{3,2,1,0:T(2,128)S(1)}, u32[]{:S(2)}, u32[]{:S(2)}) async-start(f32[16,2,2,256]{3,2,1,0:T(2,128)} %stack.2), calls=%async_computation.1 | async-start | bytes 131072 | tf_op jit(solution)/shard_map/all_to_all | solution.py:16
  79.8 8.2 %all-to-all-done.1 = f32[16,2,2,256]{3,2,1,0:T(2,128)S(1)} async-done(((f32[16,2,2,256]{3,2,1,0:T(2,128)}), f32[16,2,2,256]{3,2,1,0:T(2,128)S(1)}, u32[]{:S(2)}, u32[]{:S(2)}) %all-to-all-start.1) | async-done | bytes 65568 | tf_op jit(solution)/shard_map/all_to_all | solution.py:16
  88.1 16.2 %all-gather.5.cloned.1.call-done = bf16[576,4096]{1,0:T(8,128)(2,1)} async-done(((bf16[576,256]{1,0:T(8,128)(2,1)}), bf16[576,4096]{1,0:T(8,128)(2,1)}) %all-gather.5.cloned.1.call-update) | async-done | bytes 4718608 | tf_op jit(solution)/shard_map/all_gather | solution.py:43
  104.2 3.1 %fusion.30 = f32[512]{0:T(512)S(1)} fusion(bf16[576,4096]{1,0:T(8,128)(2,1)} %all-gather.5.cloned.1.call-done), kind=kLoop, calls=%fused_computation.47 | loop fusion | flops 6290944 | bytes 4196352 | tf_op jit(solution)/shard_map/reduce_sum | solution.py:87
  107.3 3.4 %fusion.34 = bf16[512,4096]{1,0:T(8,128)(2,1)S(1)} fusion(f32[4096]{0:T(1024)S(1)} %bitcast.216, f32[4096]{0:T(1024)S(1)} %bitcast.215, f32[4096]{0:T(1024)S(1)} %bitcast.212, f32[512]{0:T(512)S(1)} %add_rsqrt_fusion.4, bf16[576,4096]{1,0:T(8,128)(2,1)} %all-gather.5.cloned.1.call-done), kind=kLoop, calls=%fused_computation.51 | loop fusion | flops 12582912 | bytes 8439808 | tf_op jit(solution)/shard_map/convert_element_type | solution.py:88
  110.8 1.5 convolution_convert_fusion
  117.4 1.8 fusion.66
  119.7 1.5 convolution_convert_fusion.1
  121.3 3.7 %fusion.67 = f32[512,128]{0,1:T(8,128)S(1)} fusion(bf16[512,4096]{1,0:T(8,128)(2,1)} %copy-done.1, bf16[4096,128]{1,0:T(8,128)(2,1)S(1)} %copy-done.4), kind=kOutput, calls=%fused_computation.130 | convolution fusion | flops 536870912 | bytes 5505024 | tf_op jit(solution)/shard_map/dot_general | solution.py:124
  125.2 31.0 %all_gather.17 = bf16[1024,256]{1,0:T(8,128)(2,1)S(1)} all-gather(bf16[64,256]{1,0:T(8,128)(2,1)S(1)} %pad_maximum_fusion.4), channel_id=1, replica_groups=mesh['grp'=2,'sp'=16,'tp'=16] {'sp'}, dimensions={0}, use_global_device_ids=true | all-gather | bytes 557056 | tf_op jit(solution)/shard_map/all_gather | solution.py:43
  156.3 3.5 %while.36 = (s32[]{:T(128)}, f32[512,1,2]{0,2,1:T(2,128)S(1)}, f32[512,1,2]{0,2,1:T(2,128)S(1)}, f32[512,1,2,128]{0,3,2,1:T(8,128)S(1)}, bf16[1024,128]{1,0:T(8,...) while((s32[]{:T(128)}, f32[512,1,2]{0,2,1:T(2,128)S(1)}, ...), condition=%wide.region_8.9_spmd.clone, body=%wide.region_5.8_spmd.clone.sunk | while | flops 205920256 | bytes 8323255 | solution.py:180
  159.8 27.9 %all-gather.7.cloned.1.call-done = bf16[8192,256]{0,1:T(8,128)(2,1)} async-done(((bf16[512,256]{0,1:T(8,128)(2,1)}), bf16[8192,256]{0,1:T(8,128)(2,1)}) %all-gather.7.cloned.1.call-update) | async-done | bytes 4194320 | tf_op jit(solution)/shard_map/all_gather | solution.py:43
  187.7 4.6 %fusion.63 = (bf16[8192,128]{0,1:T(8,128)(2,1)}, bf16[8192,128]{0,1:T(8,128)(2,1)}) fusion(bf16[8192,256]{0,1:T(8,128)(2,1)} %all-gather.7.cloned.1.call-done), kind=kLoop, calls=%fused_computation.126 | loop fusion | bytes 8388608 | tf_op jit(solution)/shard_map/slice | solution.py:45
  192.2 54.4 %while.35 = (s32[]{:T(128)}, f32[512,1,2]{0,2,1:T(2,128)S(1)}, f32[512,1,2]{0,2,1:T(2,128)S(1)}, f32[512,1,2,128]{0,3,2,1:T(8,128)S(1)}, bf16[8192,128]{0,1:T(8,...) while((s32[]{:T(128)}, f32[512,1,2]{0,2,1:T(2,128)S(1)}, ...), condition=%wide.region_13.14_spmd, body=%wide.region_10.13_spmd.sunk | while | flops 205786112 | bytes 8061091 | solution.py:180
  194.1 1.5 fusion.98
  197.5 1.5 fusion.98
  200.9 1.5 fusion.98
  204.3 1.5 fusion.98
  207.7 1.5 fusion.98
  211.1 1.5 fusion.98
  217.9 1.5 fusion.98
  221.3 1.5 fusion.98
  224.7 1.5 fusion.98
  231.5 1.5 fusion.98
  234.9 1.5 fusion.98
  238.3 1.5 fusion.98
  245.1 1.5 fusion.98
  247.6 48.9 %all-gather.9.cloned.1.call-done = bf16[512,2048]{0,1:T(8,128)(2,1)} async-done(((bf16[512,128]{0,1:T(8,128)(2,1)}), bf16[512,2048]{0,1:T(8,128)(2,1)}) %all-gather.9.cloned.1.call-update) | async-done | bytes 2097168 | tf_op jit(solution)/shard_map/all_gather | solution.py:198
  296.5 3.0 fusion.36
  (187 shorter events, 47.0 us)
Async XLA Ops:
  6.5 289.9 %copy-start = (bf16[2048,256]{1,0:T(8,128)(2,1)S(1)}, bf16[2048,256]{1,0:T(8,128)(2,1)}, u32[]{:S(2)}) copy-start(bf16[2048,256]{1,0:T(8,128)(2,1)} %param.29) | copy-start | bytes 3145732
  6.6 48.9 %copy-start.6 = (f32[256]{0:T(256)S(1)}, f32[256]{0:T(256)}, u32[]{:S(2)}) copy-start(f32[256]{0:T(256)} %param.21) | copy-start | bytes 3076
  6.6 97.7 %all-gather.5.cloned.1.call-start = ((), (), s32[]{:S(2)}) async-start(), calls=%async_computation.2 | async-start | bytes 5013504 | tf_op jit(solution)/shard_map/all_gather | solution.py:43
  11.2 63.2 %all-to-all-start = ((f32[16,2,3,256]{3,1,2,0:T(2,128)}), f32[16,2,3,256]{3,1,2,0:T(2,128)S(1)}, u32[]{:S(2)}, u32[]{:S(2)}) async-start(f32[16,2,3,256]{3,1,2,0:T(2,128)} %broadcast_in_dim.16), calls=%async_computation | async-start | bytes 196608 | tf_op jit(solution)/shard_map/all_to_all | solution.py:31
  75.1 12.9 %all-to-all-start.1 = ((f32[16,2,2,256]{3,2,1,0:T(2,128)}), f32[16,2,2,256]{3,2,1,0:T(2,128)S(1)}, u32[]{:S(2)}, u32[]{:S(2)}) async-start(f32[16,2,2,256]{3,2,1,0:T(2,128)} %stack.2), calls=%async_computation.1 | async-start | bytes 131072 | tf_op jit(solution)/shard_map/all_to_all | solution.py:16
  79.5 108.2 %all-gather.7.cloned.1.call-start = ((), (), s32[]{:S(2)}) async-start(), calls=%async_computation.3 | async-start | bytes 4456448 | tf_op jit(solution)/shard_map/all_gather | solution.py:43
  107.3 3.4 %copy-start.2 = (bf16[4096,128]{1,0:T(8,128)(2,1)S(1)}, bf16[4096,128]{1,0:T(8,128)(2,1)}, u32[]{:S(2)}) copy-start(bf16[4096,128]{1,0:T(8,128)(2,1)} %param.24) | copy-start | bytes 3145732
  110.8 2.0 copy-start.1
  110.8 2.0 copy-start.3
  112.8 1.6 copy-start.7
  115.3 181.2 %all-gather.9.cloned.1.call-start = ((), (), s32[]{:S(2)}) async-start(), calls=%async_computation.4 | async-start | bytes 2228224 | tf_op jit(solution)/shard_map/all_gather | solution.py:198
  119.7 1.6 copy-start.4
  121.3 3.8 %copy-start.8 = (f32[64]{0:T(128)S(1)}, f32[64]{0:T(128)}, u32[]{:S(2)}) copy-start(f32[64]{0:T(128)} %param.25) | copy-start | bytes 772
  192.2 54.5 %copy-start.9 = (f32[128]{0:T(128)S(1)}, f32[128]{0:T(128)}, u32[]{:S(2)}) copy-start(f32[128]{0:T(128)} %param.28) | copy-start | bytes 1540
  192.2 104.2 %copy-start.5 = (bf16[512,256]{1,0:T(8,128)(2,1)S(1)}, bf16[512,256]{1,0:T(8,128)(2,1)}, u32[]{:S(2)}) copy-start(bf16[512,256]{1,0:T(8,128)(2,1)} %param.17) | copy-start | bytes 786436
Sparse Core Ops, SparseCore 0:
  9.4 94.7 all-gather.4
  115.4 72.1 all-gather.6
  247.7 48.7 all-gather.8
